TPU v7x, 32 devices: a whole 2x2x4 slice. The times are simulated.
32 devices in a mesh: grp: 2 (over y), sp: 4 (over z), tp: 4 (over x, core).
Axes of the slice: x: 2, y: 2, z: 4, core: 2. Of those that a mesh axis runs over, the one named last changes fastest.
Arguments:
- queries: bfloat16 [6144, 1024], P(('grp', 'sp'), 'tp'), parts along dimension 0, may hold values from -160 to 160
- key_rows: bfloat16 [6144, 256], P(('grp', 'sp'), 'tp'), parts along dimension 0, may hold values from -4 to 4
- value_rows: bfloat16 [6144, 256], P(('grp', 'sp'), 'tp'), parts along dimension 0, may hold values from -5 to 5
- sink_logits: float32 [16], P('tp'), may hold values from 2 to 6
- out_weight: bfloat16 [1024, 2048], replicated, may hold values from -0.75 to 0.75
- residual: bfloat16 [6144, 2048], P(('grp', 'sp', 'tp')), parts along dimension 0, may hold values from -6 to 6
- norm_gain: float32 [2048], replicated, may hold values from 0.1 to 1.9
- up_weight: bfloat16 [2048, 4096], P('sp', 'tp'), may hold values from -0.125 to 0.125
- down_weight: bfloat16 [4096, 2048], P('tp', 'sp'), may hold values from -0.09375 to 0.09375
Outputs:
- layer_out: bfloat16 [6144, 2048], P(('grp', 'sp', 'tp')), parts along dimension 0
There are 2 independent parts, one for each index of `grp`. A program takes and returns all parts, laid end to end along the dimension named above; an argument that names none is the same for every part. Nothing has to cross between parts.
All inputs are finite; a program needn't handle non-finite values.
Results may differ from a plain program's by a relative error of at most 0.017.
Values may be sent and summed in bfloat16 or wider, within the bound.
A program may use at most 64 MiB of HBM per device.

v0:
```python
import jax
import jax.numpy as jnp
from jax import lax
from jax.sharding import PartitionSpec as P

HEAD_DIM = 64
WINDOW = 128


def shifted(value, axis, steps):
    count = lax.axis_size(axis)
    leading, last = (max(0, -steps), min(count, count - steps))
    return lax.ppermute(value, axis, [(source, source + steps) for source in range(leading, last)])


def band_attend(queries, key_rows, value_rows, sink_logits, tail_keys, tail_values, offset):
    rows = queries.shape[0]
    kv_heads = key_rows.shape[1] // HEAD_DIM
    group = queries.shape[1] // (kv_heads * HEAD_DIM)
    blocks = rows // WINDOW
    all_keys = jnp.concatenate([tail_keys, key_rows], axis=0).reshape(
        blocks + 1, WINDOW, kv_heads, HEAD_DIM
    )
    all_values = jnp.concatenate([tail_values, value_rows], axis=0).reshape(
        blocks + 1, WINDOW, kv_heads, HEAD_DIM
    )
    key_blocks = jnp.concatenate([all_keys[:-1], all_keys[1:]], axis=1)
    value_blocks = jnp.concatenate([all_values[:-1], all_values[1:]], axis=1)
    query_blocks = queries.reshape(blocks, WINDOW, kv_heads, group, HEAD_DIM)
    scores = jnp.einsum(
        "nqkgd,nskd->nkgqs", query_blocks, key_blocks, preferred_element_type=jnp.float32
    ) * HEAD_DIM ** (-0.5)
    q_local = jnp.arange(WINDOW, dtype=jnp.int32) + WINDOW
    k_local = jnp.arange(2 * WINDOW, dtype=jnp.int32)
    distance = q_local[:, None] - k_local[None, :]
    key_position = (
        offset + (jnp.arange(blocks, dtype=jnp.int32)[:, None] - 1) * WINDOW + k_local[None, :]
    )
    valid = ((distance >= 0) & (distance < WINDOW))[None] & (key_position >= 0)[:, None, :]
    scores = jnp.where(valid[:, None, None], scores, -1e30)
    sink = sink_logits.reshape(kv_heads, group)[None, :, :, None, None]
    top = jnp.maximum(jnp.max(scores, axis=-1, keepdims=True), sink)
    weights = jnp.exp(scores - top)
    total = jnp.sum(weights, axis=-1, keepdims=True) + jnp.exp(sink - top)
    probs = (weights / total).astype(jnp.bfloat16)
    result = jnp.einsum(
        "nkgqs,nskd->nqkgd", probs, value_blocks, preferred_element_type=jnp.float32
    )
    return result.astype(jnp.bfloat16).reshape(rows, kv_heads * group * HEAD_DIM)


def body(
    queries,
    key_rows,
    value_rows,
    sink_logits,
    out_weight,
    residual,
    norm_gain,
    up_weight,
    down_weight,
):
    rows = queries.shape[0]
    width = key_rows.shape[1]
    kv_pair = jnp.concatenate([key_rows[rows - WINDOW :], value_rows[rows - WINDOW :]], axis=1)
    tail = shifted(kv_pair, "sp", 1)
    offset = lax.axis_index("sp") * rows
    attended = band_attend(
        queries, key_rows, value_rows, sink_logits, tail[:, :width], tail[:, width:], offset
    )
    head_cols = attended.shape[1]
    own_rows = lax.dynamic_slice_in_dim(out_weight, lax.axis_index("tp") * head_cols, head_cols, 0)
    projected = lax.psum_scatter(
        jnp.dot(attended, own_rows, preferred_element_type=jnp.float32).astype(jnp.bfloat16),
        "tp",
        scatter_dimension=0,
        tiled=True,
    ).astype(jnp.float32)
    mixed32 = (residual.astype(jnp.float32) + projected).astype(jnp.bfloat16).astype(jnp.float32)
    scale = lax.rsqrt(jnp.mean(mixed32 * mixed32, axis=-1, keepdims=True) + 1e-06)
    normed = (mixed32 * scale * norm_gain).astype(jnp.bfloat16)
    all_rows = lax.all_gather(normed, "tp", axis=0, tiled=True)
    before = jnp.dot(
        all_rows,
        lax.all_gather(up_weight, "sp", axis=0, tiled=True),
        preferred_element_type=jnp.float32,
    )
    hidden = jnp.square(jax.nn.relu(before)).astype(jnp.bfloat16)
    terms = jnp.dot(
        hidden,
        lax.all_gather(down_weight, "sp", axis=1, tiled=True),
        preferred_element_type=jnp.float32,
    )
    down = lax.psum_scatter(
        terms.astype(jnp.bfloat16), "tp", scatter_dimension=0, tiled=True
    ).astype(jnp.float32)
    return (mixed32 + down).astype(jnp.bfloat16)


def solution(mesh):
    in_specs = (
        P(("grp", "sp"), "tp"),
        P(("grp", "sp"), "tp"),
        P(("grp", "sp"), "tp"),
        P("tp"),
        P(),
        P(("grp", "sp", "tp"), None),
        P(),
        P("sp", "tp"),
        P("tp", "sp"),
    )
    out_specs = P(("grp", "sp", "tp"), None)
    return jax.shard_map(body, mesh=mesh, in_specs=in_specs, out_specs=out_specs, check_vma=False)
```

profile of v0, /device:TPU:0, one launch (start us, length us, event | category | flops | bytes accessed | tf_op | source)
XLA Modules:
  0.0 278.1 jit_solution(6048597584942686161)
XLA Ops:
  7.4 0.0 reduce-scatter.3.cloned.1.call-start
  7.4 0.7 slice.32
  8.1 0.7 slice.33
  8.8 4.9 %collective-permute-start = (bf16[128,128]{0,1:T(8,128)(2,1)S(1)}, bf16[128,128]{0,1:T(8,128)(2,1)S(1)}, u32[]{:S(2)}, u32[]{:S(2)}) collective-permute-start(bf16[128,128]{0,1:T(8,128)(2,1)S(1)} %pad_maximum_fusion.2), channel_id=1, source_target_pairs={{0,4},{4,8},{8,12},{1,5},{5,9},{9,13},{2,6},{6,10},{10,14},{3,7},{... | collective-permute-start | bytes 98312 | tf_op jit(solution)/shard_map/ppermute | solution.py:13
  13.8 0.1 add_compare_fusion
  13.9 0.3 broadcast_and_fusion
  14.2 1.0 slice.41
  15.2 1.0 slice.37
  16.3 1.8 reshape.128
  18.1 0.0 copy-start.3
  18.2 0.0 collective-permute-done
  18.2 0.9 pad_maximum_fusion
  19.1 0.1 slice.40
  19.3 0.1 slice.36
  19.5 0.7 fusion.1
  20.2 0.0 copy-done.3
  20.2 0.1 broadcast_maximum_fusion
  20.3 0.7 fusion
  21.0 0.1 exponential_add_fusion
  21.1 0.9 fusion.12
  22.0 0.3 copy.19
  22.3 4.0 %convolution_convert_fusion.1 = bf16[768,2048]{1,0:T(8,128)(2,1)} fusion(bf16[1024,2048]{1,0:T(8,128)(2,1)} %param.13, s32[]{:T(128)S(6)} %select_n.8, bf16[32,8,6,128]{3,2,1,0:T(8,128)(2,1)S(1)} %bitcast.60), kind=kOutput, calls=%fused_computation.1 | convolution fusion | flops 806879232 | bytes 4587524 | tf_op jit(solution)/shard_map/dot_general | solution.py:74
  26.3 0.0 copy-start
  26.3 0.0 copy-start.2
  26.3 0.0 reduce-scatter.3.cloned.1.call-update
  26.3 0.0 all-gather.6.cloned.1.call-start
  26.4 0.5 all-gather.6.cloned.1.call-update
  26.9 0.0 all-gather.8.cloned.1.call-start
  27.0 0.5 all-gather.8.cloned.1.call-update
  27.5 0.0 all-gather.4.cloned.1.call-start
  27.5 37.0 %reduce-scatter.3.cloned.1.call-done = bf16[192,2048]{1,0:T(8,128)(2,1)} async-done(((bf16[768,2048]{1,0:T(8,128)(2,1)}), bf16[192,2048]{1,0:T(8,128)(2,1)}) %reduce-scatter.3.cloned.1.call-update) | async-done | bytes 786448 | tf_op jit(solution)/shard_map/reduce_scatter | solution.py:73
  64.6 0.0 copy-done
  64.6 1.5 fusion.2
  66.1 0.0 copy-done.2
  66.1 2.3 fusion.4
  68.4 0.0 all-gather.4.cloned.1.call-update
  68.4 0.0 reduce-scatter.5.cloned.1.call-start
  68.5 40.8 %all-gather.6.cloned.1.call-done = bf16[2048,1024]{1,0:T(8,128)(2,1)} async-done(((bf16[512,1024]{1,0:T(8,128)(2,1)}), bf16[2048,1024]{1,0:T(8,128)(2,1)}) %all-gather.6.cloned.1.call-update) | async-done | bytes 4194320 | tf_op jit(solution)/shard_map/all_gather | solution.py:85
  109.2 80.6 %all-gather.8.cloned.1.call-done = bf16[1024,2048]{1,0:T(8,128)(2,1)} async-done(((bf16[1024,512]{1,0:T(8,128)(2,1)}), bf16[1024,2048]{1,0:T(8,128)(2,1)}) %all-gather.8.cloned.1.call-update) | async-done | bytes 4194320 | tf_op jit(solution)/shard_map/all_gather | solution.py:91
  189.8 28.3 %all-gather.4.cloned.1.call-done = bf16[768,2048]{1,0:T(8,128)(2,1)} async-done(((bf16[192,2048]{1,0:T(8,128)(2,1)}), bf16[768,2048]{1,0:T(8,128)(2,1)}) %all-gather.4.cloned.1.call-update) | async-done | bytes 3145744 | tf_op jit(solution)/shard_map/all_gather | solution.py:82
  218.1 11.9 %convolution_convert_fusion = bf16[768,2048]{1,0:T(8,128)(2,1)} fusion(bf16[1024,2048]{1,0:T(8,128)(2,1)} %all-gather.8.cloned.1.call-done, bf16[768,2048]{1,0:T(8,128)(2,1)} %all-gather.4.cloned.1.call-done, bf16[2048,1024]{1,0:T(8,128)(2,1)} %all-gather.6.cloned.1.call-done), kind=kOutput, calls=%fused_computation | convolution fusion | flops 6446383104 | bytes 14680064 | tf_op jit(solution)/shard_map/dot_general | solution.py:89
  230.0 0.0 copy-start.1
  230.0 0.0 reduce-scatter.5.cloned.1.call-update
  230.0 38.0 %reduce-scatter.5.cloned.1.call-done = bf16[192,2048]{1,0:T(8,128)(2,1)} async-done(((bf16[768,2048]{1,0:T(8,128)(2,1)}), bf16[192,2048]{1,0:T(8,128)(2,1)}) %reduce-scatter.5.cloned.1.call-update) | async-done | bytes 786448 | tf_op jit(solution)/shard_map/reduce_scatter | solution.py:94
  268.1 0.0 copy-done.1
  268.1 2.4 fusion.5
  (10 shorter events, 0.1 us)
Async XLA Ops:
  7.4 57.2 %reduce-scatter.3.cloned.1.call-start = ((), (), s32[]{:S(2)}) async-start(), calls=%async_computation.2 | async-start | bytes 3932160 | tf_op jit(solution)/shard_map/reduce_scatter | solution.py:73
  8.8 9.3 %collective-permute-start = (bf16[128,128]{0,1:T(8,128)(2,1)S(1)}, bf16[128,128]{0,1:T(8,128)(2,1)S(1)}, u32[]{:S(2)}, u32[]{:S(2)}) collective-permute-start(bf16[128,128]{0,1:T(8,128)(2,1)S(1)} %pad_maximum_fusion.2), channel_id=1, source_target_pairs={{0,4},{4,8},{8,12},{1,5},{5,9},{9,13},{2,6},{6,10},{10,14},{3,7},{... | collective-permute-start | bytes 98312 | tf_op jit(solution)/shard_map/ppermute | solution.py:13
  18.1 2.0 copy-start.3
  26.3 38.3 %copy-start = (bf16[192,2048]{1,0:T(8,128)(2,1)S(1)}, bf16[192,2048]{1,0:T(8,128)(2,1)}, u32[]{:S(2)}) copy-start(bf16[192,2048]{1,0:T(8,128)(2,1)} %param.14) | copy-start | bytes 2359300
  26.3 39.8 %copy-start.2 = (f32[2048]{0:T(1024)S(1)}, f32[2048]{0:T(1024)}, u32[]{:S(2)}) copy-start(f32[2048]{0:T(1024)} %param.15) | copy-start | bytes 24580
  26.3 82.9 %all-gather.6.cloned.1.call-start = ((), (), s32[]{:S(2)}) async-start(), calls=%async_computation.4 | async-start | bytes 5242880 | tf_op jit(solution)/shard_map/all_gather | solution.py:85
  26.9 162.9 %all-gather.8.cloned.1.call-start = ((), (), s32[]{:S(2)}) async-start(), calls=%async_computation.5 | async-start | bytes 5242880 | tf_op jit(solution)/shard_map/all_gather | solution.py:91
  27.5 190.6 %all-gather.4.cloned.1.call-start = ((), (), s32[]{:S(2)}) async-start(), calls=%async_computation.3 | async-start | bytes 3932160 | tf_op jit(solution)/shard_map/all_gather | solution.py:82
  68.4 199.7 %reduce-scatter.5.cloned.1.call-start = ((), (), s32[]{:S(2)}) async-start(), calls=%async_computation.6 | async-start | bytes 3932160 | tf_op jit(solution)/shard_map/reduce_scatter | solution.py:94
  230.0 38.1 %copy-start.1 = (bf16[192,2048]{1,0:T(8,128)(2,1)S(1)}, bf16[192,2048]{1,0:T(8,128)(2,1)}, u32[]{:S(2)}) copy-start(bf16[192,2048]{1,0:T(8,128)(2,1)} %reduce-scatter.3.cloned.1.call-done) | copy-start | bytes 2359300
Sparse Core Ops, SparseCore 0:
  26.4 38.0 reduce-scatter.2
  230.2 37.8 reduce-scatter.4
Sparse Core Ops, SparseCore 1:
  28.4 80.8 all-gather.5
  110.7 79.1 all-gather.7
  191.2 26.8 all-gather.3
where the time goes:
time: 279 us; the launch traced here: 278 us
  waiting for transfers between devices  226 us (81%)
  matrix products  17.5 us (6%)
  between operations  15.2 us (5%)
  other arithmetic  8.43 us (3%)
  local copies, waits for them, and re-layouts  5.95 us (2%)
  starting transfers between devices  5.11 us (2%)
    all_gather x1, waiting for transfers between devices, body(): lax.all_gather(down_weight, 'sp', axis=1, tiled=True)  80.6 us
    all_gather x1, waiting for transfers between devices, body(): lax.all_gather(up_weight, 'sp', axis=0, tiled=True)  40.8 us
    reduce_scatter x1, waiting for transfers between devices, body(): lax.psum_scatter(terms.astype(jnp.bfloat16), 'tp', scatter_dimension=0, t...  38 us
    reduce_scatter x1, waiting for transfers between devices, body(): lax.psum_scatter(jnp.dot(attended, own_rows, preferred_element_type=jnp.f...  37 us
    all_gather x1, waiting for transfers between devices, body(): all_rows = lax.all_gather(normed, 'tp', axis=0, tiled=True)  28.3 us
    dot_general x1, matrix products, body(): jnp.dot(hidden, lax.all_gather(down_weight, 'sp', axis=1, tiled=True), pr...  11.9 us
  transfers between devices with their start and end apart: 6, of which 5 were waited for; matrix products, arithmetic and copies ran while one was open for 3% of the time, Pallas kernels for 0%

commit v1 on v0

--- a/solution.py
+++ b/solution.py
@@ -1,10 +1,29 @@
+import functools
 import jax
 import jax.numpy as jnp
 from jax import lax
 from jax.sharding import PartitionSpec as P
+from jax.lax import axis_index, axis_size, ppermute
 
 HEAD_DIM = 64
 WINDOW = 128
+
+
+def match_set(field, dim_k):
+    p_count = axis_size("tp")
+    after = sorted(((s, (s + 1) % p_count) for s in range(p_count)))
+    state_now = field
+    entries = [state_now]
+    for idx in range(1, p_count):
+        state_now = ppermute(state_now, "tp", after)
+        entries.insert(0, state_now)
+    extra = jnp.concatenate(entries, axis=dim_k)
+    mat_out = axis_index("tp")
+    row_out = mat_out + 1
+    return jnp.roll(extra, row_out * field.shape[dim_k], axis=dim_k)
+
+
+widths_clear = functools.partial(match_set, dim_k=0)
 
 
 def shifted(value, axis, steps):
@@ -79,7 +98,7 @@
     mixed32 = (residual.astype(jnp.float32) + projected).astype(jnp.bfloat16).astype(jnp.float32)
     scale = lax.rsqrt(jnp.mean(mixed32 * mixed32, axis=-1, keepdims=True) + 1e-06)
     normed = (mixed32 * scale * norm_gain).astype(jnp.bfloat16)
-    all_rows = lax.all_gather(normed, "tp", axis=0, tiled=True)
+    all_rows = widths_clear(normed)
     before = jnp.dot(
         all_rows,
         lax.all_gather(up_weight, "sp", axis=0, tiled=True),

time: 279 us -> 253 us (0.907)
  waiting for transfers between devices: 226 us -> 187 us
  local copies, waits for them, and re-layouts: 5.95 us -> 18.1 us
    all_gather x1, waiting for transfers between devices: 40.8 us -> 0.01 us  [body(): lax.all_gather(up_weight, 'sp', axis=0, tiled=True)]
    ppermute x0 -> x3, waiting for transfers between devices: none -> 34.3 us  [match_set(): state_now = ppermute(state_now, 'tp', after)]
    all_gather x1 -> x0, waiting for transfers between devices: 28.3 us -> none  [body(): all_rows = lax.all_gather(normed, 'tp', axis=0, tiled=True)]
    unnamed x8 -> x15, local copies, waits for them, and re-layouts: 0.02 us -> 8.97 us
  transfers between devices with their start and end apart: 6 -> 8, of which waited for: 5 -> 6; matrix products, arithmetic and copies ran while one was open for 3% -> 7% of each run, Pallas kernels for 0% -> 0%
where the time goes in v1:
time: 253 us
  waiting for transfers between devices  187 us (74%)
  matrix products  19.5 us (8%)
  local copies, waits for them, and re-layouts  18.1 us (7%)
  between operations  15 us (6%)
  other arithmetic  8.19 us (3%)
  starting transfers between devices  5.14 us (2%)
    all_gather x1, waiting for transfers between devices, body(): lax.all_gather(down_weight, 'sp', axis=1, tiled=True)  77.9 us
    reduce_scatter x1, waiting for transfers between devices, body(): lax.psum_scatter(jnp.dot(attended, own_rows, preferred_element_type=jnp.f...  37 us
    reduce_scatter x1, waiting for transfers between devices, body(): lax.psum_scatter(terms.astype(jnp.bfloat16), 'tp', scatter_dimension=0, t...  36.5 us
    ppermute x3, waiting for transfers between devices, match_set(): state_now = ppermute(state_now, 'tp', after)  34.3 us
    dot_general x1, matrix products, body(): jnp.dot(hidden, lax.all_gather(down_weight, 'sp', axis=1, tiled=True), pr...  11.9 us
    unnamed x15, local copies, waits for them, and re-layouts  8.97 us
  transfers between devices with their start and end apart: 8, of which 6 were waited for; matrix products, arithmetic and copies ran while one was open for 7% of the time, Pallas kernels for 0%

profile of v1, /device:TPU:0, one launch (start us, length us, event | category | flops | bytes accessed | tf_op | source)
XLA Modules:
  0.0 252.8 jit_solution(9443562196966784608)
XLA Ops:
  7.4 0.7 slice.32
  8.1 0.7 slice.33
  8.8 4.9 %collective-permute-start = (bf16[128,128]{0,1:T(8,128)(2,1)S(1)}, bf16[128,128]{0,1:T(8,128)(2,1)S(1)}, u32[]{:S(2)}, u32[]{:S(2)}) collective-permute-start(bf16[128,128]{0,1:T(8,128)(2,1)S(1)} %pad_maximum_fusion.2), channel_id=1, source_target_pairs={{0,4},{4,8},{8,12},{1,5},{5,9},{9,13},{2,6},{6,10},{10,14},{3,7},{... | collective-permute-start | bytes 98312 | tf_op jit(solution)/shard_map/ppermute | solution.py:32
  13.8 0.1 add_compare_fusion
  13.9 0.3 broadcast_and_fusion
  14.2 1.0 slice.41
  15.2 1.0 slice.37
  16.3 2.5 %reshape.128 = bf16[6,128,4,64]{3,2,1,0:T(4,128)(2,1)} reshape(bf16[768,256]{1,0:T(8,128)(2,1)} %param.9) | data formatting | bytes 786432 | tf_op jit(solution)/shard_map/reshape.10
  18.8 0.6 copy.13
  19.5 0.0 collective-permute-done
  19.5 1.6 pad_maximum_fusion
  21.0 0.1 slice.40
  21.2 1.9 fusion.3
  23.1 0.1 broadcast_maximum_fusion
  23.1 0.7 fusion.2
  23.8 0.1 exponential_add_fusion
  23.9 1.0 slice.36
  25.0 1.8 fusion.16
  26.8 0.3 copy.19
  27.1 3.9 %convolution_convert_fusion.1 = bf16[768,2048]{1,0:T(8,128)(2,1)} fusion(bf16[1024,2048]{1,0:T(8,128)(2,1)} %param.13, s32[]{:T(128)S(6)} %select_n.21, bf16[32,8,6,128]{3,2,1,0:T(8,128)(2,1)S(1)} %bitcast.59), kind=kOutput, calls=%fused_computation.1 | convolution fusion | flops 806879232 | bytes 4587524 | tf_op jit(solution)/shard_map/dot_general | solution.py:93
  31.0 0.0 reduce-scatter.3.cloned.1.call-update
  31.0 0.0 all-gather.3.cloned.1.call-start
  31.1 0.5 all-gather.3.cloned.1.call-update
  31.6 0.0 all-gather.5.cloned.1.call-start
  31.6 0.5 all-gather.5.cloned.1.call-update
  32.2 0.0 reduce-scatter.5.cloned.1.call-start
  32.2 37.0 %reduce-scatter.3.cloned.1.call-done = bf16[192,2048]{1,0:T(8,128)(2,1)} async-done(((bf16[768,2048]{1,0:T(8,128)(2,1)}), bf16[192,2048]{1,0:T(8,128)(2,1)}) %reduce-scatter.3.cloned.1.call-update) | async-done | bytes 786448 | tf_op jit(solution)/shard_map/reduce_scatter | solution.py:92
  69.3 1.5 fusion.6
  70.7 1.5 fusion.8
  72.2 0.1 collective-permute-start.1
  72.3 11.4 %collective-permute-done.1 = bf16[192,2048]{1,0:T(8,128)(2,1)S(1)} collective-permute-done((bf16[192,2048]{1,0:T(8,128)(2,1)S(1)}, bf16[192,2048]{1,0:T(8,128)(2,1)S(1)}, u32[]{:S(2)}, u32[]{:S(2)}) %collective-permute-start.1) | collective-permute-done | bytes 786464 | tf_op jit(solution)/shard_map/ppermute | solution.py:18
  83.7 0.0 collective-permute-start.2
  83.7 11.4 %collective-permute-done.2 = bf16[192,2048]{1,0:T(8,128)(2,1)S(1)} collective-permute-done((bf16[192,2048]{1,0:T(8,128)(2,1)S(1)}, bf16[192,2048]{1,0:T(8,128)(2,1)S(1)}, u32[]{:S(2)}, u32[]{:S(2)}) %collective-permute-start.2) | collective-permute-done | bytes 786464 | tf_op jit(solution)/shard_map/ppermute | solution.py:18
  95.1 0.0 collective-permute-start.3
  95.1 11.5 %collective-permute-done.3 = bf16[192,2048]{1,0:T(8,128)(2,1)} collective-permute-done((bf16[192,2048]{1,0:T(8,128)(2,1)S(1)}, bf16[192,2048]{1,0:T(8,128)(2,1)}, u32[]{:S(2)}, u32[]{:S(2)}) %collective-permute-start.3) | collective-permute-done | bytes 786464 | tf_op jit(solution)/shard_map/ppermute | solution.py:18
  106.6 2.1 constant_dynamic-update-slice_fusion.7
  108.7 1.0 constant_dynamic-update-slice_fusion.6
  109.7 0.9 constant_dynamic-update-slice_fusion.5
  110.6 0.9 constant_dynamic-update-slice_fusion.4
  111.6 2.1 constant_dynamic-update-slice_fusion.3
  113.7 1.0 constant_dynamic-update-slice_fusion.2
  114.6 1.0 constant_dynamic-update-slice_fusion.1
  115.6 0.9 constant_dynamic-update-slice_fusion
  116.5 77.9 %all-gather.5.cloned.1.call-done = bf16[1024,2048]{1,0:T(8,128)(2,1)} async-done(((bf16[1024,512]{1,0:T(8,128)(2,1)}), bf16[1024,2048]{1,0:T(8,128)(2,1)}) %all-gather.5.cloned.1.call-update) | async-done | bytes 4194320 | tf_op jit(solution)/shard_map/all_gather | solution.py:110
  194.5 11.9 %convolution_convert_fusion = bf16[768,2048]{1,0:T(8,128)(2,1)} fusion(bf16[1024,2048]{1,0:T(8,128)(2,1)} %all-gather.5.cloned.1.call-done, bf16[2048,1024]{1,0:T(8,128)(2,1)} %all-gather.3.cloned.1.call-done, bf16[1536,2048]{1,0:T(8,128)(2,1)} %constant_dynamic-update-slice_fusion, s32[]{:T(128)S(6)} %select_n.23), kind=kOutput, calls=%fused_computation | convolution fusion | flops 6446383104 | bytes 14680068 | tf_op jit(solution)/shard_map/dot_general | solution.py:108
  206.4 0.0 reduce-scatter.5.cloned.1.call-update
  206.4 36.5 %reduce-scatter.5.cloned.1.call-done = bf16[192,2048]{1,0:T(8,128)(2,1)} async-done(((bf16[768,2048]{1,0:T(8,128)(2,1)}), bf16[192,2048]{1,0:T(8,128)(2,1)}) %reduce-scatter.5.cloned.1.call-update) | async-done | bytes 786448 | tf_op jit(solution)/shard_map/reduce_scatter | solution.py:113
  242.9 2.4 fusion.9
  (19 shorter events, 0.1 us)
Async XLA Ops:
  7.4 61.9 %reduce-scatter.3.cloned.1.call-start = ((), (), s32[]{:S(2)}) async-start(), calls=%async_computation.2 | async-start | bytes 3932160 | tf_op jit(solution)/shard_map/reduce_scatter | solution.py:92
  8.8 10.6 %collective-permute-start = (bf16[128,128]{0,1:T(8,128)(2,1)S(1)}, bf16[128,128]{0,1:T(8,128)(2,1)S(1)}, u32[]{:S(2)}, u32[]{:S(2)}) collective-permute-start(bf16[128,128]{0,1:T(8,128)(2,1)S(1)} %pad_maximum_fusion.2), channel_id=1, source_target_pairs={{0,4},{4,8},{8,12},{1,5},{5,9},{9,13},{2,6},{6,10},{10,14},{3,7},{... | collective-permute-start | bytes 98312 | tf_op jit(solution)/shard_map/ppermute | solution.py:32
  18.8 4.3 %copy-start.3 = (f32[4]{0:T(128)S(1)}, f32[4]{0:T(128)}, u32[]{:S(2)}) copy-start(f32[4]{0:T(128)} %param.12) | copy-start | bytes 52
  31.0 38.3 %copy-start = (bf16[192,2048]{1,0:T(8,128)(2,1)S(1)}, bf16[192,2048]{1,0:T(8,128)(2,1)}, u32[]{:S(2)}) copy-start(bf16[192,2048]{1,0:T(8,128)(2,1)} %param.14) | copy-start | bytes 2359300
  31.0 39.7 %copy-start.2 = (f32[2048]{0:T(1024)S(1)}, f32[2048]{0:T(1024)}, u32[]{:S(2)}) copy-start(f32[2048]{0:T(1024)} %param.15) | copy-start | bytes 24580
  31.0 85.5 %all-gather.3.cloned.1.call-start = ((), (), s32[]{:S(2)}) async-start(), calls=%async_computation.3 | async-start | bytes 5242880 | tf_op jit(solution)/shard_map/all_gather | solution.py:104
  31.6 162.9 %all-gather.5.cloned.1.call-start = ((), (), s32[]{:S(2)}) async-start(), calls=%async_computation.4 | async-start | bytes 5242880 | tf_op jit(solution)/shard_map/all_gather | solution.py:110
  32.2 210.7 %reduce-scatter.5.cloned.1.call-start = ((), (), s32[]{:S(2)}) async-start(), calls=%async_computation.5 | async-start | bytes 3932160 | tf_op jit(solution)/shard_map/reduce_scatter | solution.py:113
  72.2 11.5 %collective-permute-start.1 = (bf16[192,2048]{1,0:T(8,128)(2,1)S(1)}, bf16[192,2048]{1,0:T(8,128)(2,1)S(1)}, u32[]{:S(2)}, u32[]{:S(2)}) collective-permute-start(bf16[192,2048]{1,0:T(8,128)(2,1)S(1)} %fusion.8), channel_id=1, source_target_pairs={{0,1},{1,2},{2,3},{3,0},{4,5},{5,6},{6,7},{7,4},{8,9},{9,10},{10,1... | collective-permute-start | bytes 2359304 | tf_op jit(solution)/shard_map/ppermute | solution.py:18
  83.7 11.4 %collective-permute-start.2 = (bf16[192,2048]{1,0:T(8,128)(2,1)S(1)}, bf16[192,2048]{1,0:T(8,128)(2,1)S(1)}, u32[]{:S(2)}, u32[]{:S(2)}) collective-permute-start(bf16[192,2048]{1,0:T(8,128)(2,1)S(1)} %collective-permute-done.1), channel_id=1, source_target_pairs={{0,1},{1,2},{2,3},{3,0},{4,5},{5,6},{6,7},{7,4},{8,9},{9,10},{10,1... | collective-permute-start | bytes 2359304 | tf_op jit(solution)/shard_map/ppermute | solution.py:18
  95.1 11.5 %collective-permute-start.3 = (bf16[192,2048]{1,0:T(8,128)(2,1)S(1)}, bf16[192,2048]{1,0:T(8,128)(2,1)}, u32[]{:S(2)}, u32[]{:S(2)}) collective-permute-start(bf16[192,2048]{1,0:T(8,128)(2,1)S(1)} %collective-permute-done.2), channel_id=1, source_target_pairs={{0,1},{1,2},{2,3},{3,0},{4,5},{5,6},{6,7},{7,4},{8,9},{9,10},{10,1... | collective-permute-start | bytes 2359304 | tf_op jit(solution)/shard_map/ppermute | solution.py:18
  206.4 36.6 %copy-start.1 = (bf16[192,2048]{1,0:T(8,128)(2,1)S(1)}, bf16[192,2048]{1,0:T(8,128)(2,1)}, u32[]{:S(2)}) copy-start(bf16[192,2048]{1,0:T(8,128)(2,1)} %reduce-scatter.3.cloned.1.call-done) | copy-start | bytes 2359300
Sparse Core Ops, SparseCore 0:
  31.1 38.0 reduce-scatter.2
  206.5 36.3 reduce-scatter.4
Sparse Core Ops, SparseCore 1:
  33.1 80.8 all-gather.2
  115.4 79.1 all-gather.4
